TPU v7x, 32 devices: a whole 2x2x4 slice. The times are simulated.
32 devices in a mesh: sp: 8 (over z, x), tp: 4 (over y, core).
Axes of the slice: x: 2, y: 2, z: 4, core: 2. Of those that a mesh axis runs over, the one named last changes fastest.
Arguments:
- query_small: bfloat16 [6144, 1024], P('sp', 'tp'), may hold values from -18 to 18
- key_small: bfloat16 [6144, 1024], P('sp', 'tp'), may hold values from -6 to 6
- value_small: bfloat16 [6144, 1024], P('sp', 'tp'), may hold values from -6 to 6
- offset_small: bfloat16 [16, 6144], P('tp', 'sp'), may hold values from -25 to 0
- query_large: bfloat16 [6144, 1024], P('sp', 'tp'), may hold values from -18 to 18
- key_large: bfloat16 [6144, 1024], P('sp', 'tp'), may hold values from -6 to 6
- value_large: bfloat16 [6144, 1024], P('sp', 'tp'), may hold values from -6 to 6
- offset_large: bfloat16 [8, 6144], P('tp', 'sp'), may hold values from -25 to 0
- out_small: bfloat16 [1024, 2048], P('tp'), may hold values from -0.125 to 0.125
- out_large: bfloat16 [1024, 2048], P('tp'), may hold values from -0.125 to 0.125
- residual: bfloat16 [6144, 2048], P(('sp', 'tp')), may hold values from -1.1953125 to 1.1953125
- norm_gain: bfloat16 [2048], replicated, may hold values from 0.099609375 to 1.8984375
- gate_weight: bfloat16 [2048, 5632], P('sp', 'tp'), may hold values from -0.125 to 0.125
- up_weight: bfloat16 [2048, 5632], P('sp', 'tp'), may hold values from -0.125 to 0.125
- down_weight: bfloat16 [5632, 2048], P('tp', 'sp'), may hold values from -0.078125 to 0.078125
Outputs:
- layer_out: bfloat16 [6144, 2048], P(('sp', 'tp'))
All inputs are finite; a program needn't handle non-finite values.
Results may differ from a plain program's by a relative error of at most 0.023.
Values may be sent and summed in bfloat16 or wider, within the bound.
A program may use at most 128 MiB of HBM per device.

v0:
```python
import functools
import math

import jax
import jax.numpy as jnp
from jax import lax
from jax.experimental import pallas as pl
from jax.experimental.pallas import tpu as pltpu
from jax.sharding import PartitionSpec as P


SMALL_DIM = 64
LARGE_DIM = 128
TILE = 256
LANES = 128
LOG2E = math.log2(math.e)
OFFSET_ROWS = 16
MESH = pl.DeviceIdType.MESH


def dot_t(a, b):
    return lax.dot_general(a, b, (((1,), (1,)), ((), ())), preferred_element_type=jnp.float32)


def column_count(mesh):
    line = [getattr(d, "coords", None) for d in mesh.devices[:, 0].reshape(-1)]
    if line[0] is None or mesh.axis_names != ("sp", "tp"):
        return 1
    width = 1
    while width < len(line) and line[width][2] == line[0][2]:
        width += 1
    return width if len(line) % width == 0 else 1


def attend_kernel(
    n_sp,
    width,
    n_small,
    n_large,
    q_ref,
    own_ref,
    tri_ref,
    out_ref,
    qs_ref,
    acc_ref,
    carry_ref,
    kv_ref,
    local_sem,
    up_sem,
    row_sem,
    recv_sem,
):
    height = n_sp // width
    sp = lax.axis_index("sp")
    tp = lax.axis_index("tp")
    z, x = sp // width, sp % width
    tokens = q_ref.shape[0]
    tiles = tokens // TILE
    small_cols = n_small * SMALL_DIM
    n_pairs = small_cols // LANES
    large_cols = n_large * LARGE_DIM
    per_group = own_ref.shape[1] // TILE

    def send(source, block, target, send_sem):
        return pltpu.make_async_remote_copy(
            src_ref=source,
            dst_ref=kv_ref.at[block],
            send_sem=send_sem,
            recv_sem=recv_sem.at[block],
            device_id=(target, tp),
            device_id_type=MESH,
        )

    barrier = pltpu.get_barrier_semaphore()
    for other in range(n_sp):

        @pl.when(other != sp)
        def _(other=other):
            pl.semaphore_signal(barrier, inc=1, device_id=(other, tp), device_id_type=MESH)

    local = pltpu.make_async_copy(own_ref, kv_ref.at[sp], local_sem)
    local.start()
    pl.semaphore_wait(barrier, n_sp - 1)

    def sends(row, act, source=None):
        block = row * width + x
        origin = kv_ref.at[block] if source is None else source

        @pl.when(z < height - 1)
        def _():
            act(send(origin, block, sp + width, up_sem.at[row]))

        for column in range(width):

            @pl.when((column != x) & ((row < z) | (column > x)))
            def _(column=column):
                act(send(origin, block, z * width + column, row_sem.at[row, column]))

    sends(z, lambda copy: copy.start(), own_ref)

    lane = lax.broadcasted_iota(jnp.int32, (tokens, LANES), 1)
    low_rows = lane < SMALL_DIM
    low = low_rows[:TILE]
    zero = jnp.zeros((TILE, LANES), jnp.bfloat16)
    zero_rows = jnp.zeros((tokens, LANES), jnp.bfloat16)
    for pair in range(n_pairs):
        q = q_ref[:, pair * LANES : (pair + 1) * LANES]
        qs_ref[2 * pair] = jnp.where(low_rows, q, zero_rows)
        qs_ref[2 * pair + 1] = jnp.where(low_rows, zero_rows, q)
    for head in range(n_large):
        first = small_cols + head * LANES
        qs_ref[n_small + head] = q_ref[:, first : first + LANES]
    acc_ref[...] = jnp.zeros_like(acc_ref)
    carry_ref[...] = jnp.zeros_like(carry_ref)
    tri = tri_ref[...]

    def weights_of(head, q_rows, key, offset, scale, before):
        z = dot_t(qs_ref[head, q_rows, :], key) * scale + offset
        t = jnp.log(1.0 + jnp.exp2(-jnp.abs(z))) * LOG2E
        log_pass = jnp.minimum(z, 0.0) - t
        log_fail = log_pass - z
        if before is not None:
            log_fail = jnp.where(before, log_fail, 0.0)
        after = jnp.dot(log_fail.astype(jnp.bfloat16), tri, preferred_element_type=jnp.float32)
        carried = carry_ref[head, q_rows, :]
        weights = jnp.exp2(log_pass + after + carried)
        if before is not None:
            weights = jnp.where(before, weights, 0.0)
        carry_ref[head, q_rows, :] = carried + after[:, :1] + log_fail[:, :1]
        return weights.astype(jnp.bfloat16)

    def one_tile(block, q_tile, tile, before):
        q_rows = pl.ds(pl.multiple_of(q_tile * TILE, TILE), TILE)
        rows = pl.ds(pl.multiple_of(tile * TILE, TILE), TILE)
        group = pl.multiple_of(tokens + (tile // per_group) * OFFSET_ROWS, OFFSET_ROWS)
        lanes = pl.multiple_of((tile % per_group) * TILE, TILE)
        offsets = kv_ref[block, pl.ds(group, OFFSET_ROWS), pl.ds(lanes, TILE)]
        offsets = offsets.astype(jnp.float32) * LOG2E
        for pair in range(n_pairs):
            cols = slice(pair * LANES, (pair + 1) * LANES)
            v_cols = slice(small_cols + pair * LANES, small_cols + (pair + 1) * LANES)
            key = kv_ref[block, rows, cols]
            value = kv_ref[block, rows, v_cols]
            scale = LOG2E * SMALL_DIM**-0.5
            first = 2 * pair
            w0 = weights_of(first, q_rows, key, offsets[first : first + 1], scale, before)
            w1 = weights_of(first + 1, q_rows, key, offsets[first + 1 : first + 2], scale, before)
            acc_ref[q_rows, cols] += jnp.dot(
                w0, jnp.where(low, value, zero), preferred_element_type=jnp.float32
            ) + jnp.dot(w1, jnp.where(low, zero, value), preferred_element_type=jnp.float32)
        for head in range(n_large):
            k_cols = slice(2 * small_cols + head * LANES, 2 * small_cols + (head + 1) * LANES)
            v_first = 2 * small_cols + large_cols + head * LANES
            out_cols = slice(small_cols + head * LANES, small_cols + (head + 1) * LANES)
            place = n_small + head
            w = weights_of(
                place,
                q_rows,
                kv_ref[block, rows, k_cols],
                offsets[place : place + 1],
                LOG2E * LARGE_DIM**-0.5,
                before,
            )
            acc_ref[q_rows, out_cols] += jnp.dot(
                w, kv_ref[block, rows, v_first : v_first + LANES], preferred_element_type=jnp.float32
            )

    row_pos = lax.broadcasted_iota(jnp.int32, (TILE, TILE), 0)
    key_pos = lax.broadcasted_iota(jnp.int32, (TILE, TILE), 1)
    local.wait()

    def own_tile(q_tile, nothing):
        one_tile(sp, q_tile, q_tile, key_pos < row_pos)
        return nothing

    lax.fori_loop(0, tiles, own_tile, 0)

    def whole_block(block):
        def body(index, nothing):
            one_tile(block, index // tiles, tiles - 1 - index % tiles, None)
            return nothing

        lax.fori_loop(0, tiles * tiles, body, 0)

    def rest(q_tile, nothing):
        def inner(index, nothing):
            one_tile(sp, q_tile, q_tile - 1 - index, None)
            return nothing

        return lax.fori_loop(0, q_tile, inner, nothing)

    lax.fori_loop(1, tiles, rest, 0)

    def arrived(block):
        send(kv_ref.at[block], block, sp, up_sem.at[0]).wait_recv()

    def one_row(index, nothing):
        row = z - index

        @pl.when(index > 0)
        def _():
            arrived(row * width + x)
            sends(row, lambda copy: copy.start())

        def one_column(step, nothing):
            column = width - 1 - step
            block = row * width + column

            @pl.when((index > 0) | (column < x))
            def _():
                @pl.when(column != x)
                def _():
                    arrived(block)

                whole_block(block)

            return nothing

        return lax.fori_loop(0, width, one_column, nothing)

    lax.fori_loop(0, z + 1, one_row, 0)
    out_ref[...] = acc_ref[...].astype(jnp.bfloat16)

    def finish(row, nothing):
        sends(row, lambda copy: copy.wait_send())
        return nothing

    lax.fori_loop(0, z + 1, finish, 0)


def attend(n_sp, width, query, packed, n_small, n_large):
    tokens, cols = query.shape
    heads = n_small + n_large
    height = n_sp // width
    places = jnp.arange(TILE, dtype=jnp.int32)
    tri = (places[:, None] > places[None, :]).astype(jnp.bfloat16)
    vmem = pl.BlockSpec(memory_space=pltpu.VMEM)
    return pl.pallas_call(
        functools.partial(attend_kernel, n_sp, width, n_small, n_large),
        out_shape=jax.ShapeDtypeStruct((tokens, cols), jnp.bfloat16),
        in_specs=[vmem, pl.BlockSpec(memory_space=pl.ANY), vmem],
        out_specs=vmem,
        scratch_shapes=[
            pltpu.VMEM((heads, tokens, LANES), jnp.bfloat16),
            pltpu.VMEM((tokens, cols), jnp.float32),
            pltpu.VMEM((heads, tokens, 1), jnp.float32),
            pltpu.VMEM((n_sp,) + packed.shape, jnp.bfloat16),
            pltpu.SemaphoreType.DMA,
            pltpu.SemaphoreType.DMA((height,)),
            pltpu.SemaphoreType.DMA((height, width)),
            pltpu.SemaphoreType.DMA((n_sp,)),
        ],
        compiler_params=pltpu.CompilerParams(
            vmem_limit_bytes=48 * 1024 * 1024, collective_id=0, has_side_effects=True
        ),
        cost_estimate=pl.CostEstimate(
            flops=2 * 3 * heads * tokens * tokens * n_sp * TILE,
            bytes_accessed=8 * n_sp * tokens * cols,
            transcendentals=3 * heads * tokens * tokens * n_sp,
        ),
        name="stick_attend",
    )(query, packed, tri)


def pack(keys_values, offsets):
    rows = jnp.concatenate(keys_values, axis=1)
    tokens, cols = rows.shape
    heads = offsets.shape[0]
    groups = -(-tokens // (cols // TILE * TILE))
    span = cols // TILE * TILE
    flat = jnp.pad(offsets, ((0, OFFSET_ROWS - heads), (0, groups * span - tokens)))
    flat = flat.reshape(OFFSET_ROWS, groups, span).transpose(1, 0, 2)
    flat = flat.reshape(groups * OFFSET_ROWS, span)
    return jnp.concatenate([rows, jnp.pad(flat, ((0, 0), (0, cols - span)))], axis=0)


def rounded(value):
    return lax.optimization_barrier(value.astype(jnp.bfloat16)).astype(jnp.float32)


def rms_norm(stream, gain):
    scale = lax.rsqrt(jnp.mean(stream * stream, axis=-1, keepdims=True) + 1e-06)
    return (stream * scale * gain.astype(jnp.float32)).astype(jnp.bfloat16)


def on_device(n_sp, width, *args):
    return layer(n_sp, width, *args)


def layer(
    n_sp,
    width,
    query_small,
    key_small,
    value_small,
    offset_small,
    query_large,
    key_large,
    value_large,
    offset_large,
    out_small,
    out_large,
    residual,
    norm_gain,
    gate_weight,
    up_weight,
    down_weight,
):
    packed = pack(
        (key_small, value_small, key_large, value_large),
        jnp.concatenate([offset_small, offset_large], axis=0),
    )
    gate_full = lax.all_gather(gate_weight, "sp", axis=0, tiled=True)
    up_full = lax.all_gather(up_weight, "sp", axis=0, tiled=True)
    down_full = lax.all_gather(down_weight, "sp", axis=1, tiled=True)
    query = jnp.concatenate([query_small, query_large], axis=1)
    out_rows = jnp.concatenate([out_small, out_large], axis=0)
    mixed = attend(
        n_sp, width, query, packed, offset_small.shape[0], offset_large.shape[0]
    )
    attended = lax.psum_scatter(
        jnp.dot(mixed, out_rows, preferred_element_type=jnp.float32).astype(jnp.bfloat16),
        "tp",
        scatter_dimension=0,
        tiled=True,
    ).astype(jnp.float32)
    stream = residual.astype(jnp.float32) + rounded(attended)
    normed = rms_norm(stream, norm_gain)
    normed_rows = lax.all_gather(normed, "tp", axis=0, tiled=True)
    gate = jnp.dot(normed_rows, gate_full, preferred_element_type=jnp.float32)
    upper = jnp.dot(normed_rows, up_full, preferred_element_type=jnp.float32)
    hidden = (jax.nn.silu(gate) * upper).astype(jnp.bfloat16)
    summed = lax.psum_scatter(
        jnp.dot(hidden, down_full, preferred_element_type=jnp.float32).astype(jnp.bfloat16),
        "tp",
        scatter_dimension=0,
        tiled=True,
    ).astype(jnp.float32)
    return (stream + rounded(summed)).astype(jnp.bfloat16)


def solution(mesh):
    return jax.shard_map(
        functools.partial(on_device, mesh.shape["sp"], column_count(mesh)),
        mesh=mesh,
        in_specs=(
            P("sp", "tp"),
            P("sp", "tp"),
            P("sp", "tp"),
            P("tp", "sp"),
            P("sp", "tp"),
            P("sp", "tp"),
            P("sp", "tp"),
            P("tp", "sp"),
            P("tp", None),
            P("tp", None),
            P(("sp", "tp"), None),
            P(),
            P("sp", "tp"),
            P("sp", "tp"),
            P("tp", "sp"),
        ),
        out_specs=P(("sp", "tp"), None),
        check_vma=False,
    )
```

profile of v0, /device:TPU:16, one launch (start us, length us, event | category | flops | bytes accessed | tf_op | source)
XLA Modules:
  0.0 624.5 jit_solution(17254503325668630223)
XLA Ops:
  7.4 0.0 reduce-scatter.3.cloned.1.call-start
  7.4 0.7 fusion.9
  8.1 1.2 pad_maximum_fusion.1.q_ref
  9.3 1.6 pad_maximum_fusion.own_ref
  10.9 0.0 copy-start.3
  10.9 0.0 copy-start.4
  10.9 156.5 %stick_attend.1 = bf16[768,512]{1,0:T(8,128)(2,1)S(1)} custom-call(bf16[768,512]{1,0:T(8,128)(2,1)S(1)} %pad_maximum_fusion.1.q_ref, bf16[784,1024]{1,0:T(8,128)(2,1)S(1)} %pad_maximum_fusion.own_ref, bf16[256,256]{1,0:T(8,128)(2,1)S(1)} %fusion.3.tri_ref), custom_call_target="tpu_custom_call" | custom-call | flops 43486543872 | bytes 25165824 | tf_op jit(solution)/shard_map/stick_attend/pallas_call | solution.py:238
  167.4 0.0 copy-done.3
  167.4 3.5 convolution_convert_fusion
  170.9 0.0 reduce-scatter.3.cloned.1.call-update
  171.0 0.0 all-gather.7.cloned.1.call-start
  171.0 0.5 all-gather.7.cloned.1.call-update
  171.5 0.0 all-gather.5.cloned.1.call-start
  171.6 0.0 copy-done.2
  171.6 117.7 %reduce-scatter.3.cloned.1.call-done = bf16[192,2048]{1,0:T(8,128)(2,1)} async-done(((bf16[768,2048]{1,0:T(8,128)(2,1)}), bf16[192,2048]{1,0:T(8,128)(2,1)}) %reduce-scatter.3.cloned.1.call-update) | async-done | bytes 786448 | tf_op jit(solution)/shard_map/reduce_scatter | solution.py:321
  289.3 1.5 multiply_reduce_fusion
  290.8 2.3 multiply_convert_fusion.1
  293.1 0.0 all-gather.5.cloned.1.call-update
  293.1 0.0 all-gather.11.cloned.1.call-start
  293.2 0.5 all-gather.11.cloned.1.call-update
  293.7 0.0 all-gather.9.cloned.1.call-start
  293.8 0.7 all-gather.9.cloned.1.call-update
  294.5 0.2 reduce-scatter.5.cloned.1.call-start
  294.7 50.5 %all-gather.7.cloned.1.call-done = bf16[2048,1408]{1,0:T(8,128)(2,1)} async-done(((bf16[256,1408]{1,0:T(8,128)(2,1)}), bf16[2048,1408]{1,0:T(8,128)(2,1)}) %all-gather.7.cloned.1.call-update) | async-done | bytes 5767184 | tf_op jit(solution)/shard_map/all_gather | solution.py:313
  345.2 28.9 %all-gather.5.cloned.1.call-done = bf16[768,2048]{1,0:T(8,128)(2,1)} async-done(((bf16[192,2048]{1,0:T(8,128)(2,1)}), bf16[768,2048]{1,0:T(8,128)(2,1)}) %all-gather.5.cloned.1.call-update) | async-done | bytes 3145744 | tf_op jit(solution)/shard_map/all_gather | solution.py:329
  374.1 9.7 %fusion.12 = f32[768,1408]{1,0:T(8,128)} fusion(bf16[768,2048]{1,0:T(8,128)(2,1)} %all-gather.5.cloned.1.call-done, bf16[2048,1408]{1,0:T(8,128)(2,1)} %all-gather.7.cloned.1.call-done), kind=kOutput, calls=%fused_computation.25 | convolution fusion | flops 4429185024 | bytes 13238272 | tf_op jit(solution)/shard_map/dot_general | solution.py:330
  383.8 84.2 %all-gather.11.cloned.1.call-done = bf16[1408,2048]{1,0:T(8,128)(2,1)} async-done(((bf16[1408,256]{1,0:T(8,128)(2,1)}), bf16[1408,2048]{1,0:T(8,128)(2,1)}) %all-gather.11.cloned.1.call-update) | async-done | bytes 5767184 | tf_op jit(solution)/shard_map/all_gather | solution.py:315
  468.0 92.5 %all-gather.9.cloned.1.call-done = bf16[2048,1408]{1,0:T(8,128)(2,1)} async-done(((bf16[256,1408]{1,0:T(8,128)(2,1)}), bf16[2048,1408]{1,0:T(8,128)(2,1)}) %all-gather.9.cloned.1.call-update) | async-done | bytes 5767184 | tf_op jit(solution)/shard_map/all_gather | solution.py:314
  560.5 16.8 %convolution_convert_fusion.1 = bf16[768,2048]{1,0:T(8,128)(2,1)} fusion(bf16[1408,2048]{1,0:T(8,128)(2,1)} %all-gather.11.cloned.1.call-done, f32[768,1408]{1,0:T(8,128)} %fusion.12, bf16[768,2048]{1,0:T(8,128)(2,1)} %all-gather.5.cloned.1.call-done, bf16[2048,1408]{1,0:T(8,128)(2,1)} %all-gather.9.cloned.1.call-done), kind=kOutput, calls=%fused_computation.2 | convolution fusion | flops 8866430976 | bytes 22151168 | tf_op jit(solution)/shard_map/dot_general | solution.py:334
  577.3 0.0 reduce-scatter.5.cloned.1.call-update
  577.4 37.1 %reduce-scatter.5.cloned.1.call-done = bf16[192,2048]{1,0:T(8,128)(2,1)} async-done(((bf16[768,2048]{1,0:T(8,128)(2,1)}), bf16[192,2048]{1,0:T(8,128)(2,1)}) %reduce-scatter.5.cloned.1.call-update) | async-done | bytes 786448 | tf_op jit(solution)/shard_map/reduce_scatter | solution.py:333
  614.5 2.4 add_convert_fusion
  (9 shorter events, 0.0 us)
Async XLA Ops:
  7.4 281.9 %reduce-scatter.3.cloned.1.call-start = ((), (), s32[]{:S(2)}) async-start(), calls=%async_computation.2 | async-start | bytes 3932160 | tf_op jit(solution)/shard_map/reduce_scatter | solution.py:321
  10.9 156.5 %copy-start.3 = (bf16[256,2048]{1,0:T(8,128)(2,1)S(1)}, bf16[256,2048]{1,0:T(8,128)(2,1)}, u32[]{:S(2)}) copy-start(bf16[256,2048]{1,0:T(8,128)(2,1)} %param.24) | copy-start | bytes 3145732
  10.9 156.5 %copy-start.4 = (bf16[256,2048]{1,0:T(8,128)(2,1)S(1)}, bf16[256,2048]{1,0:T(8,128)(2,1)}, u32[]{:S(2)}) copy-start(bf16[256,2048]{1,0:T(8,128)(2,1)} %param.23) | copy-start | bytes 3145732
  170.9 0.7 copy-start.2
  170.9 118.4 %copy-start = (bf16[192,2048]{1,0:T(8,128)(2,1)S(1)}, bf16[192,2048]{1,0:T(8,128)(2,1)}, u32[]{:S(2)}) copy-start(bf16[192,2048]{1,0:T(8,128)(2,1)} %param.25) | copy-start | bytes 2359300
  171.0 174.2 %all-gather.7.cloned.1.call-start = ((), (), s32[]{:S(2)}) async-start(), calls=%async_computation.4 | async-start | bytes 6488064 | tf_op jit(solution)/shard_map/all_gather | solution.py:313
  171.5 202.6 %all-gather.5.cloned.1.call-start = ((), (), s32[]{:S(2)}) async-start(), calls=%async_computation.3 | async-start | bytes 3932160 | tf_op jit(solution)/shard_map/all_gather | solution.py:329
  293.1 174.9 %all-gather.11.cloned.1.call-start = ((), (), s32[]{:S(2)}) async-start(), calls=%async_computation.6 | async-start | bytes 6488064 | tf_op jit(solution)/shard_map/all_gather | solution.py:315
  293.7 266.8 %all-gather.9.cloned.1.call-start = ((), (), s32[]{:S(2)}) async-start(), calls=%async_computation.5 | async-start | bytes 6488064 | tf_op jit(solution)/shard_map/all_gather | solution.py:314
  294.5 320.0 %reduce-scatter.5.cloned.1.call-start = ((), (), s32[]{:S(2)}) async-start(), calls=%async_computation.7 | async-start | bytes 3932160 | tf_op jit(solution)/shard_map/reduce_scatter | solution.py:333
  577.3 37.1 %copy-start.1 = (bf16[192,2048]{1,0:T(8,128)(2,1)S(1)}, bf16[192,2048]{1,0:T(8,128)(2,1)}, u32[]{:S(2)}) copy-start(bf16[192,2048]{1,0:T(8,128)(2,1)} %reduce-scatter.3.cloned.1.call-done) | copy-start | bytes 2359300
Sparse Core Ops, SparseCore 0:
  171.1 118.1 reduce-scatter.2
  577.5 36.9 reduce-scatter.4
Sparse Core Ops, SparseCore 1:
  173.6 171.5 all-gather.6
  346.6 27.5 all-gather.4
  376.0 92.0 all-gather.10
  470.2 90.2 all-gather.8
where the time goes:
time: 626 us; the launch traced here: 624 us
  waiting for transfers between devices  413 us (66%)
  Pallas kernels  157 us (25%)
  matrix products  30 us (5%)
  between operations  15.1 us (2%)
  other arithmetic  9.69 us (2%)
    pallas_call x1, Pallas kernels, attend(): pl.pallas_call(functools.partial(attend_kernel, n_sp, width, n_small, n_l...  157 us
    reduce_scatter x1, waiting for transfers between devices, layer(): lax.psum_scatter(jnp.dot(mixed, out_rows, preferred_element_type=jnp.floa...  118 us
    all_gather x1, waiting for transfers between devices, layer(): up_full = lax.all_gather(up_weight, 'sp', axis=0, tiled=True)  92.5 us
    all_gather x1, waiting for transfers between devices, layer(): down_full = lax.all_gather(down_weight, 'sp', axis=1, tiled=True)  84.2 us
    all_gather x1, waiting for transfers between devices, layer(): gate_full = lax.all_gather(gate_weight, 'sp', axis=0, tiled=True)  50.5 us
    reduce_scatter x1, waiting for transfers between devices, layer(): lax.psum_scatter(jnp.dot(hidden, down_full, preferred_element_type=jnp.fl...  37.1 us
    all_gather x1, waiting for transfers between devices, layer(): normed_rows = lax.all_gather(normed, 'tp', axis=0, tiled=True)  28.9 us
    dot_general x1, matrix products, layer(): jnp.dot(hidden, down_full, preferred_element_type=jnp.float32)  16.8 us
  transfers between devices with their start and end apart: 6, of which 6 were waited for; matrix products, arithmetic and copies ran while one was open for 2% of the time, Pallas kernels for 0%

commit v1 on v0

--- a/solution.py
+++ b/solution.py
@@ -32,105 +32,63 @@
     return width if len(line) % width == 0 else 1
 
 
-def attend_kernel(
-    n_sp,
+def stick_attention(
     width,
     n_small,
     n_large,
-    q_ref,
-    own_ref,
+    small_ref,
+    large_ref,
     tri_ref,
-    out_ref,
     qs_ref,
     acc_ref,
     carry_ref,
     kv_ref,
-    local_sem,
-    up_sem,
-    row_sem,
-    recv_sem,
+    own_ready,
+    arrived,
+    forward,
+    landed,
 ):
-    height = n_sp // width
     sp = lax.axis_index("sp")
-    tp = lax.axis_index("tp")
     z, x = sp // width, sp % width
-    tokens = q_ref.shape[0]
+    tokens = small_ref.shape[0]
     tiles = tokens // TILE
     small_cols = n_small * SMALL_DIM
     n_pairs = small_cols // LANES
     large_cols = n_large * LARGE_DIM
-    per_group = own_ref.shape[1] // TILE
-
-    def send(source, block, target, send_sem):
-        return pltpu.make_async_remote_copy(
-            src_ref=source,
-            dst_ref=kv_ref.at[block],
-            send_sem=send_sem,
-            recv_sem=recv_sem.at[block],
-            device_id=(target, tp),
-            device_id_type=MESH,
-        )
-
-    barrier = pltpu.get_barrier_semaphore()
-    for other in range(n_sp):
-
-        @pl.when(other != sp)
-        def _(other=other):
-            pl.semaphore_signal(barrier, inc=1, device_id=(other, tp), device_id_type=MESH)
-
-    local = pltpu.make_async_copy(own_ref, kv_ref.at[sp], local_sem)
-    local.start()
-    pl.semaphore_wait(barrier, n_sp - 1)
-
-    def sends(row, act, source=None):
-        block = row * width + x
-        origin = kv_ref.at[block] if source is None else source
-
-        @pl.when(z < height - 1)
-        def _():
-            act(send(origin, block, sp + width, up_sem.at[row]))
-
-        for column in range(width):
-
-            @pl.when((column != x) & ((row < z) | (column > x)))
-            def _(column=column):
-                act(send(origin, block, z * width + column, row_sem.at[row, column]))
-
-    sends(z, lambda copy: copy.start(), own_ref)
-
+    per_group = kv_ref.shape[2] // TILE
     lane = lax.broadcasted_iota(jnp.int32, (tokens, LANES), 1)
     low_rows = lane < SMALL_DIM
     low = low_rows[:TILE]
     zero = jnp.zeros((TILE, LANES), jnp.bfloat16)
     zero_rows = jnp.zeros((tokens, LANES), jnp.bfloat16)
     for pair in range(n_pairs):
-        q = q_ref[:, pair * LANES : (pair + 1) * LANES]
+        q = small_ref[:, pair * LANES : (pair + 1) * LANES]
         qs_ref[2 * pair] = jnp.where(low_rows, q, zero_rows)
         qs_ref[2 * pair + 1] = jnp.where(low_rows, zero_rows, q)
     for head in range(n_large):
-        first = small_cols + head * LANES
-        qs_ref[n_small + head] = q_ref[:, first : first + LANES]
+        qs_ref[n_small + head] = large_ref[:, head * LANES : (head + 1) * LANES]
     acc_ref[...] = jnp.zeros_like(acc_ref)
     carry_ref[...] = jnp.zeros_like(carry_ref)
-    tri = tri_ref[...]
+    source = lax.broadcasted_iota(jnp.int32, (TILE, TILE), 0)
+    target = lax.broadcasted_iota(jnp.int32, (TILE, TILE), 1)
+    tri_ref[...] = (source > target).astype(jnp.bfloat16)
 
     def weights_of(head, q_rows, key, offset, scale, before):
         z = dot_t(qs_ref[head, q_rows, :], key) * scale + offset
-        t = jnp.log(1.0 + jnp.exp2(-jnp.abs(z))) * LOG2E
-        log_pass = jnp.minimum(z, 0.0) - t
-        log_fail = log_pass - z
+        soft = jnp.maximum(jnp.log(1.0 + jnp.exp2(jnp.minimum(z, 126.0))) * LOG2E, z)
+        log_pass = z - soft
         if before is not None:
-            log_fail = jnp.where(before, log_fail, 0.0)
-        after = jnp.dot(log_fail.astype(jnp.bfloat16), tri, preferred_element_type=jnp.float32)
+            soft = jnp.where(before, soft, 0.0)
+        after = jnp.dot(soft.astype(jnp.bfloat16), tri_ref[...], preferred_element_type=jnp.float32)
         carried = carry_ref[head, q_rows, :]
-        weights = jnp.exp2(log_pass + after + carried)
+        weights = jnp.exp2(log_pass - (after + carried))
         if before is not None:
             weights = jnp.where(before, weights, 0.0)
-        carry_ref[head, q_rows, :] = carried + after[:, :1] + log_fail[:, :1]
+        carry_ref[head, q_rows, :] = carried + after[:, :1] + soft[:, :1]
         return weights.astype(jnp.bfloat16)
 
-    def one_tile(block, q_tile, tile, before):
-        q_rows = pl.ds(pl.multiple_of(q_tile * TILE, TILE), TILE)
+    def one_tile(block, q_tile, tile, before, count=TILE):
+        q_rows = pl.ds(pl.multiple_of(q_tile * TILE, TILE), count)
         rows = pl.ds(pl.multiple_of(tile * TILE, TILE), TILE)
         group = pl.multiple_of(tokens + (tile // per_group) * OFFSET_ROWS, OFFSET_ROWS)
         lanes = pl.multiple_of((tile % per_group) * TILE, TILE)
@@ -167,7 +125,7 @@
 
     row_pos = lax.broadcasted_iota(jnp.int32, (TILE, TILE), 0)
     key_pos = lax.broadcasted_iota(jnp.int32, (TILE, TILE), 1)
-    local.wait()
+    own_ready()
 
     def own_tile(q_tile, nothing):
         one_tile(sp, q_tile, q_tile, key_pos < row_pos)
@@ -177,10 +135,10 @@
 
     def whole_block(block):
         def body(index, nothing):
-            one_tile(block, index // tiles, tiles - 1 - index % tiles, None)
+            one_tile(block, 0, tiles - 1 - index, None, tokens)
             return nothing
 
-        lax.fori_loop(0, tiles * tiles, body, 0)
+        lax.fori_loop(0, tiles, body, 0)
 
     def rest(q_tile, nothing):
         def inner(index, nothing):
@@ -191,16 +149,19 @@
 
     lax.fori_loop(1, tiles, rest, 0)
 
-    def arrived(block):
-        send(kv_ref.at[block], block, sp, up_sem.at[0]).wait_recv()
+    def next_row(row):
+        @pl.when(row > 0)
+        def _():
+            arrived((row - 1) * width + x)
+            forward(row - 1)
+
+    @pl.when(x == 0)
+    def _():
+        next_row(z)
 
     def one_row(index, nothing):
         row = z - index
-
-        @pl.when(index > 0)
-        def _():
-            arrived(row * width + x)
-            sends(row, lambda copy: copy.start())
+        first_other = jnp.where(index == 0, x, jnp.where(x == width - 1, x, width)) - 1
 
         def one_column(step, nothing):
             column = width - 1 - step
@@ -211,6 +172,11 @@
                 @pl.when(column != x)
                 def _():
                     arrived(block)
+                    landed(block)
+
+                @pl.when(column == first_other)
+                def _():
+                    next_row(row)
 
                 whole_block(block)
 
@@ -219,28 +185,129 @@
         return lax.fori_loop(0, width, one_column, nothing)
 
     lax.fori_loop(0, z + 1, one_row, 0)
+
+
+class Travel:
+    def __init__(self, n_sp, width, own_ref, kv_ref, up_sem, row_sem, recv_sem, shifted):
+        self.shifted = shifted
+        self.n_sp, self.width = n_sp, width
+        self.own_ref, self.kv_ref = own_ref, kv_ref
+        self.up_sem, self.row_sem, self.recv_sem = up_sem, row_sem, recv_sem
+        self.sp, self.tp = lax.axis_index("sp"), lax.axis_index("tp")
+        self.z, self.x = self.sp // width, self.sp % width
+
+    def send(self, source, block, target, send_sem):
+        return pltpu.make_async_remote_copy(
+            src_ref=source,
+            dst_ref=self.kv_ref.at[block],
+            send_sem=send_sem,
+            recv_sem=self.recv_sem.at[block],
+            device_id=(target, self.tp),
+            device_id_type=MESH,
+        )
+
+    def sends(self, row, act, source=None):
+        block = row * self.width + self.x
+        origin = self.kv_ref.at[block] if source is None else source
+
+        @pl.when(self.z < self.n_sp // self.width - 1)
+        def _():
+            act(self.send(origin, block, self.sp + self.width, self.up_sem.at[row]))
+
+        for column in range(self.width):
+
+            wanted = (column != self.x) & ((row < self.z) | (column > self.x))
+            if self.shifted:
+                wanted &= (row > 0) | (self.z == 0) | (self.x > 0)
+
+            @pl.when(wanted)
+            def _(column=column):
+                target = self.z * self.width + column
+                act(self.send(origin, block, target, self.row_sem.at[row, column]))
+
+    def start_own(self):
+        self.sends(self.z, lambda copy: copy.start(), self.own_ref)
+
+    def forward(self, row):
+        self.sends(row, lambda copy: copy.start())
+
+    def arrived(self, block):
+        self.send(self.kv_ref.at[block], block, self.sp, self.up_sem.at[0]).wait_recv()
+
+    def finish(self):
+        def one(row, nothing):
+            self.sends(row, lambda copy: copy.wait_send())
+            return nothing
+
+        lax.fori_loop(0, self.z + 1, one, 0)
+
+
+def attend_kernel(
+    n_sp,
+    width,
+    n_small,
+    n_large,
+    small_ref,
+    large_ref,
+    own_ref,
+    out_ref,
+    tri_ref,
+    qs_ref,
+    acc_ref,
+    carry_ref,
+    kv_ref,
+    local_sem,
+    up_sem,
+    row_sem,
+    recv_sem,
+):
+    travel = Travel(n_sp, width, own_ref, kv_ref, up_sem, row_sem, recv_sem, False)
+    barrier = pltpu.get_barrier_semaphore()
+    for other in range(n_sp):
+
+        @pl.when(other != travel.sp)
+        def _(other=other):
+            pl.semaphore_signal(
+                barrier, inc=1, device_id=(other, travel.tp), device_id_type=MESH
+            )
+
+    local = pltpu.make_async_copy(own_ref, kv_ref.at[travel.sp], local_sem)
+    local.start()
+    pl.semaphore_wait(barrier, n_sp - 1)
+    travel.start_own()
+    stick_attention(
+        width,
+        n_small,
+        n_large,
+        small_ref,
+        large_ref,
+        tri_ref,
+        qs_ref,
+        acc_ref,
+        carry_ref,
+        kv_ref,
+        local.wait,
+        travel.arrived,
+        travel.forward,
+        lambda block: None,
+    )
     out_ref[...] = acc_ref[...].astype(jnp.bfloat16)
-
-    def finish(row, nothing):
-        sends(row, lambda copy: copy.wait_send())
-        return nothing
-
-    lax.fori_loop(0, z + 1, finish, 0)
-
-
-def attend(n_sp, width, query, packed, n_small, n_large):
-    tokens, cols = query.shape
+    travel.finish()
+
+
+def attend(n_sp, width, query_small, query_large, packed, n_small, n_large):
+    tokens = query_small.shape[0]
+    cols = query_small.shape[1] + query_large.shape[1]
     heads = n_small + n_large
     height = n_sp // width
-    places = jnp.arange(TILE, dtype=jnp.int32)
-    tri = (places[:, None] > places[None, :]).astype(jnp.bfloat16)
     vmem = pl.BlockSpec(memory_space=pltpu.VMEM)
     return pl.pallas_call(
         functools.partial(attend_kernel, n_sp, width, n_small, n_large),
         out_shape=jax.ShapeDtypeStruct((tokens, cols), jnp.bfloat16),
-        in_specs=[vmem, pl.BlockSpec(memory_space=pl.ANY), vmem],
+        in_specs=[vmem, vmem, pl.BlockSpec(memory_space=pl.ANY)],
         out_specs=vmem,
         scratch_shapes=[
+            pltpu.VMEM((TILE, TILE), jnp.bfloat16),
             pltpu.VMEM((heads, tokens, LANES), jnp.bfloat16),
             pltpu.VMEM((tokens, cols), jnp.float32),
             pltpu.VMEM((heads, tokens, 1), jnp.float32),
@@ -259,7 +326,7 @@
             transcendentals=3 * heads * tokens * tokens * n_sp,
         ),
         name="stick_attend",
-    )(query, packed, tri)
+    )(query_small, query_large, packed)
 
 
 def pack(keys_values, offsets):
@@ -281,6 +348,481 @@
 def rms_norm(stream, gain):
     scale = lax.rsqrt(jnp.mean(stream * stream, axis=-1, keepdims=True) + 1e-06)
     return (stream * scale * gain.astype(jnp.float32)).astype(jnp.bfloat16)
+
+
+def fits(n_sp, width, tokens, hidden):
+    return (
+        lax.axis_size("tp") == 4
+        and width == 2
+        and n_sp % 4 == 0
+        and hidden % LANES == 0
+        and tokens % (4 * OFFSET_ROWS) == 0
+    )
+
+
+def layer_kernel(
+    n_sp,
+    width,
+    n_small,
+    n_large,
+    small_ref,
+    large_ref,
+    own_ref,
+    out_small_ref,
+    out_large_ref,
+    residual_ref,
+    gain_ref,
+    gate_ref,
+    up_ref,
+    down_ref,
+    out_ref,
+    tri_ref,
+    qs_ref,
+    acc_ref,
+    carry_ref,
+    kv_ref,
+    wg_ref,
+    wu_ref,
+    wd_ref,
+    mixed_ref,
+    core_out_ref,
+    core_in_ref,
+    side_out_ref,
+    side_in_ref,
+    normed_ref,
+    stream_ref,
+    swap_out_ref,
+    swap_in_ref,
+    sum_ref,
+    sum_in_ref,
+    local_sem,
+    up_sem,
+    row_sem,
+    recv_sem,
+    shift_sem,
+    own_w_sem,
+    column_w_sem,
+    row_w_sem,
+    recv_w_sem,
+    core_sem,
+    side_sem,
+    gather_sem,
+    pass_sem,
+    gather_in_sem,
+    swap_sem,
+    sum_sem,
+):
+    travel = Travel(n_sp, width, own_ref, kv_ref, up_sem, row_sem, recv_sem, True)
+    height = n_sp // width
+    sp, tp, z, x = travel.sp, travel.tp, travel.z, travel.x
+    y, core = tp // 2, tp % 2
+    partner = y * 2 + 1 - core
+    across = (1 - y) * 2 + core
+    low = z % 2
+    z_other = z - low + 1 - low
+    depth = gate_ref.shape[0]
+    share = wg_ref.shape[1]
+    spare = gate_ref.shape[1] - share
+    part = residual_ref.shape[0]
+
+    barrier = pltpu.get_barrier_semaphore()
+    for other in range(n_sp):
+
+        @pl.when(other != sp)
+        def _(other=other):
+            pl.semaphore_signal(barrier, inc=1, device_id=(other, tp), device_id_type=MESH)
+
+    for other in range(4):
+
+        @pl.when(other != tp)
+        def _(other=other):
+            pl.semaphore_signal(barrier, inc=1, device_id=(sp, other), device_id_type=MESH)
+
+    corner = z_other * width + x
+    pl.semaphore_signal(barrier, inc=1, device_id=(corner, across), device_id_type=MESH)
+
+    local = pltpu.make_async_copy(own_ref, kv_ref.at[sp], local_sem)
+    local.start()
+
+    def weight_ends(block, half):
+        first = pl.multiple_of(half * spare, LANES)
+        rows = pl.ds(pl.multiple_of(block * depth, depth), depth)
+        return (
+            (gate_ref.at[:, pl.ds(first, share)], wg_ref.at[rows, :]),
+            (up_ref.at[:, pl.ds(first, share)], wu_ref.at[rows, :]),
+            (down_ref.at[pl.ds(first, share), :], wd_ref.at[:, rows]),
+        )
+
+    own_weights = tuple(
+        pltpu.make_async_copy(source, target, own_w_sem.at[i])
+        for i, (source, target) in enumerate(weight_ends(sp, low))
+    )
+    for copy in own_weights:
+        copy.start()
+    pl.semaphore_wait(barrier, n_sp - 1 + 3 + 1)
+    travel.start_own()
+
+    def weight_copies(block, half, target, send_sems, held):
+        return tuple(
+            pltpu.make_async_remote_copy(
+                src_ref=place if held else source,
+                dst_ref=place,
+                send_sem=send_sems.at[i],
+                recv_sem=recv_w_sem.at[block, i],
+                device_id=(target, tp),
+                device_id_type=MESH,
+            )
+            for i, (source, place) in enumerate(weight_ends(block, half))
+        )
+
+    def column_weights(row, act):
+        for copy in weight_copies(sp, row % 2, row * width + x, column_w_sem.at[row], False):
+            act(copy)
+
+    def row_weights(row, act, held):
+        target = z * width + 1 - x
+        for copy in weight_copies(row * width + x, low, target, row_w_sem.at[row], held):
+            act(copy)
+
+    def start(copy):
+        copy.start()
+
+    def wait_send(copy):
+        copy.wait_send()
+
+    def wait_recv(copy):
+        copy.wait_recv()
+
+    def weights_down(index, nothing):
+        column_weights(z - 1 - index, start)
+        return nothing
+
+    lax.fori_loop(0, z, weights_down, 0)
+
+    def pass_on(row):
+        for copy in weight_copies(row * width + x, low, sp, column_w_sem.at[row], True):
+            wait_recv(copy)
+        row_weights(row, start, True)
+
+    def from_above(index, nothing):
+        pass_on(z + 1 + index)
+        return nothing
+
+    def last_sends():
+        @pl.when(z < height - 1)
+        def _():
+            column_weights(z + 1, start)
+
+        row_weights(z, start, False)
+        lax.fori_loop(0, height - 1 - z, from_above, 0)
+
+    def shift_copy():
+        return travel.send(kv_ref.at[0], 0, sp + width, shift_sem)
+
+    @pl.when(sp == 0)
+    def _():
+        last_sends()
+
+    def forward(row):
+        travel.forward(row)
+
+        @pl.when((row == 0) & (x == 0))
+        def _():
+            last_sends()
+
+    def landed(block):
+        @pl.when((block == 0) & (x == 1))
+        def _():
+            @pl.when(z < height - 1)
+            def _():
+                shift_copy().start()
+
+            last_sends()
+
+    stick_attention(
+        width,
+        n_small,
+        n_large,
+        small_ref,
+        large_ref,
+        tri_ref,
+        qs_ref,
+        acc_ref,
+        carry_ref,
+        kv_ref,
+        local.wait,
+        travel.arrived,
+        forward,
+        landed,
+    )
+    mixed_ref[...] = acc_ref[...].astype(jnp.bfloat16)
+
+    small_cols = out_small_ref.shape[0]
+
+    def chunk_product(chunk):
+        rows = pl.ds(pl.multiple_of(chunk * part, OFFSET_ROWS), part)
+        return jnp.dot(
+            mixed_ref[rows, :small_cols], out_small_ref[...], preferred_element_type=jnp.float32
+        ) + jnp.dot(
+            mixed_ref[rows, small_cols:], out_large_ref[...], preferred_element_type=jnp.float32
+        )
+
+    def to(place, block, source, target, send_sem, arrive_sem):
+        return pltpu.make_async_remote_copy(
+            src_ref=source,
+            dst_ref=target,
+            send_sem=send_sem,
+            recv_sem=arrive_sem,
+            device_id=(place, block),
+            device_id_type=MESH,
+        )
+
+    core_copies = tuple(
+        to(sp, partner, core_out_ref.at[i], core_in_ref.at[i], core_sem.at[0, i], core_sem.at[1, i])
+        for i in range(2)
+    )
+    side_copy = to(sp, across, side_out_ref, side_in_ref, side_sem.at[0], side_sem.at[1])
+    core_out_ref[0] = chunk_product((1 - y) * 2 + 1 - core).astype(jnp.bfloat16)
+    core_copies[0].start()
+    stream_ref[...] = chunk_product(across)
+    core_copies[0].wait_recv()
+    side_out_ref[...] = (stream_ref[...] + core_in_ref[0].astype(jnp.float32)).astype(jnp.bfloat16)
+    side_copy.start()
+    core_out_ref[1] = chunk_product(y * 2 + 1 - core).astype(jnp.bfloat16)
+    core_copies[1].start()
+    stream_ref[...] = chunk_product(tp)
+    core_copies[1].wait_recv()
+    stream_ref[...] += core_in_ref[1].astype(jnp.float32)
+    side_copy.wait_recv()
+    attended = (stream_ref[...] + side_in_ref[...].astype(jnp.float32)).astype(jnp.bfloat16)
+    stream = residual_ref[...].astype(jnp.float32) + attended.astype(jnp.float32)
+    stream_ref[...] = stream
+    scale = lax.rsqrt(jnp.mean(stream * stream, axis=-1, keepdims=True) + 1e-06)
+    my_rows = pl.ds(pl.multiple_of(core * part, OFFSET_ROWS), part)
+    other_rows = pl.ds(pl.multiple_of((1 - core) * part, OFFSET_ROWS), part)
+    my_chip = low * 2 + y
+    normed_ref[my_chip, my_rows, :] = (
+        stream_ref[...] * scale * gain_ref[...].astype(jnp.float32)
+    ).astype(jnp.bfloat16)
+
+    def chip_of(step):
+        dz, dy = 1 - step // 2, 1 - step % 2
+        low_there = (low + dz) % 2
+        y_there = (y + dy) % 2
+        place = (z - low + low_there) * width + x
+        return low_there * 2 + y_there, place, y_there * 2 + core
+
+    def spread(step):
+        _, place, block = chip_of(step)
+        here = normed_ref.at[my_chip, my_rows, :]
+        return to(place, block, here, here, gather_sem.at[step], gather_in_sem.at[my_chip, 0])
+
+    def to_partner(chip, step):
+        here = normed_ref.at[chip, my_rows, :]
+        return to(sp, partner, here, here, pass_sem.at[step], gather_in_sem.at[chip, 1])
+
+    def from_partner(chip):
+        here = normed_ref.at[chip, other_rows, :]
+        return to(sp, partner, here, here, pass_sem.at[0], gather_in_sem.at[chip, 1])
+
+    for step in (2, 1, 0):
+        spread(step).start()
+    to_partner(my_chip, 3).start()
+
+    def far_up(index, nothing):
+        column_weights(height - 1 - index, start)
+        return nothing
+
+    def from_below(index, nothing):
+        pass_on(z - 1 - index)
+        return nothing
+
+    lax.fori_loop(0, height - 2 - z, far_up, 0)
+    lax.fori_loop(0, z, from_below, 0)
+    for step in (2, 1, 0):
+        chip, _, _ = chip_of(step)
+        here = normed_ref.at[chip, my_rows, :]
+        to(sp, partner, here, here, gather_sem.at[step], gather_in_sem.at[chip, 0]).wait_recv()
+        to_partner(chip, step).start()
+
+    for copy in own_weights:
+        copy.wait()
+
+    def row_arrived(row, nothing):
+        for copy in weight_copies(row * width + 1 - x, low, sp, row_w_sem.at[row], True):
+            wait_recv(copy)
+        return nothing
+
+    lax.fori_loop(0, height, row_arrived, 0)
+    place_of = lax.broadcasted_iota(jnp.int32, (2 * part, share), 1)
+    counted = place_of >= low * (share - spare)
+
+    def swap_copy(step):
+        return to(
+            sp, partner, swap_out_ref.at[step], swap_in_ref.at[step], swap_sem.at[0, step], swap_sem.at[1, step]
+        )
+
+    def sum_copy(step):
+        _, place, block = chip_of(step)
+        return to(place, block, sum_ref.at[step], sum_in_ref.at[step], sum_sem.at[0, step], sum_sem.at[1, step])
+
+    def add_partner(step):
+        swap_copy(step).wait_recv()
+        total = sum_ref[step].astype(jnp.float32) + swap_in_ref[step].astype(jnp.float32)
+        sum_ref[step] = total.astype(jnp.bfloat16)
+
+    def feed(step, nothing):
+        chip, _, _ = chip_of(step)
+        from_partner(chip).wait_recv()
+        rows = normed_ref[chip]
+        gate = jnp.dot(rows, wg_ref[...], preferred_element_type=jnp.float32)
+        upper = jnp.dot(rows, wu_ref[...], preferred_element_type=jnp.float32)
+        hidden = jnp.where(counted, jax.nn.silu(gate) * upper, 0.0).astype(jnp.bfloat16)
+        down = jnp.dot(hidden, wd_ref[...], preferred_element_type=jnp.float32)
+        first = down[:part].astype(jnp.bfloat16)
+        second = down[part:].astype(jnp.bfloat16)
+
+        @pl.when(core == 0)
+        def _():
+            sum_ref[step] = first
+            swap_out_ref[step] = second
+
+        @pl.when(core == 1)
+        def _():
+            sum_ref[step] = second
+            swap_out_ref[step] = first
+
+        swap_copy(step).start()
+
+        @pl.when(step > 0)
+        def _():
+            add_partner(step - 1)
+            sum_copy(step - 1).start()
+
+        return nothing
+
+    lax.fori_loop(0, 4, feed, 0)
+    add_partner(3)
+    total = sum_ref[3].astype(jnp.float32)
+    for step in range(3):
+        sum_copy(step).wait_recv()
+        total += sum_in_ref[step].astype(jnp.float32)
+    mixer = total.astype(jnp.bfloat16).astype(jnp.float32)
+    out_ref[...] = (stream_ref[...] + mixer).astype(jnp.bfloat16)
+
+    travel.finish()
+
+    @pl.when((x == 1) & (z < height - 1))
+    def _():
+        shift_copy().wait_send()
+
+    for copy in core_copies:
+        wait_send(copy)
+    wait_send(side_copy)
+    for step in range(3):
+        wait_send(spread(step))
+        wait_send(sum_copy(step))
+    for step in range(4):
+        wait_send(to_partner(my_chip, step))
+        wait_send(swap_copy(step))
+
+    def weights_sent(row, nothing):
+        @pl.when(row != z)
+        def _():
+            column_weights(row, wait_send)
+
+        row_weights(row, wait_send, True)
+        return nothing
+
+    lax.fori_loop(0, height, weights_sent, 0)
+
+
+def fused_layer(
+    n_sp,
+    width,
+    query_small,
+    query_large,
+    packed,
+    n_small,
+    n_large,
+    out_small,
+    out_large,
+    residual,
+    norm_gain,
+    gate_weight,
+    up_weight,
+    down_weight,
+):
+    tokens = query_small.shape[0]
+    cols = query_small.shape[1] + query_large.shape[1]
+    heads = n_small + n_large
+    height = n_sp // width
+    part, model = residual.shape
+    hidden = gate_weight.shape[1]
+    share = -(-hidden // (2 * LANES)) * LANES
+    vmem = pl.BlockSpec(memory_space=pltpu.VMEM)
+    hbm = pl.BlockSpec(memory_space=pl.ANY)
+    piece = (part, model)
+    bf16 = jnp.bfloat16
+    dma = pltpu.SemaphoreType.DMA
+    return pl.pallas_call(
+        functools.partial(layer_kernel, n_sp, width, n_small, n_large),
+        out_shape=jax.ShapeDtypeStruct(piece, bf16),
+        in_specs=[vmem, vmem, hbm, vmem, vmem, vmem, vmem, hbm, hbm, hbm],
+        out_specs=vmem,
+        scratch_shapes=[
+            pltpu.VMEM((TILE, TILE), bf16),
+            pltpu.VMEM((heads, tokens, LANES), bf16),
+            pltpu.VMEM((tokens, cols), jnp.float32),
+            pltpu.VMEM((heads, tokens, 1), jnp.float32),
+            pltpu.VMEM((n_sp,) + packed.shape, bf16),
+            pltpu.VMEM((model, share), bf16),
+            pltpu.VMEM((model, share), bf16),
+            pltpu.VMEM((share, model), bf16),
+            pltpu.VMEM((tokens, cols), bf16),
+            pltpu.VMEM((2,) + piece, bf16),
+            pltpu.VMEM((2,) + piece, bf16),
+            pltpu.VMEM(piece, bf16),
+            pltpu.VMEM(piece, bf16),
+            pltpu.VMEM((4, 2 * part, model), bf16),
+            pltpu.VMEM(piece, jnp.float32),
+            pltpu.VMEM((4,) + piece, bf16),
+            pltpu.VMEM((4,) + piece, bf16),
+            pltpu.VMEM((4,) + piece, bf16),
+            pltpu.VMEM((3,) + piece, bf16),
+            dma,
+            dma((height,)),
+            dma((height, width)),
+            dma((n_sp,)),
+            dma,
+            dma((3,)),
+            dma((height, 3)),
+            dma((height, 3)),
+            dma((n_sp, 3)),
+            dma((2, 2)),
+            dma((2,)),
+            dma((3,)),
+            dma((4,)),
+            dma((4, 2)),
+            dma((2, 4)),
+            dma((2, 3)),
+        ],
+        compiler_params=pltpu.CompilerParams(
+            vmem_limit_bytes=67043328, collective_id=1, has_side_effects=True
+        ),
+        name="fused_layer",
+    )(
+        query_small,
+        query_large,
+        packed,
+        out_small,
+        out_large,
+        residual,
+        norm_gain.reshape(1, model),
+        gate_weight,
+        up_weight,
+        down_weight,
+    )
 
 
 def on_device(n_sp, width, *args):
@@ -306,6 +848,26 @@
     up_weight,
     down_weight,
 ):
+    if fits(n_sp, width, value_small.shape[0], gate_weight.shape[1]):
+        return fused_layer(
+            n_sp,
+            width,
+            query_small,
+            query_large,
+            pack(
+                (key_small, value_small, key_large, value_large),
+                jnp.concatenate([offset_small, offset_large], axis=0),
+            ),
+            offset_small.shape[0],
+            offset_large.shape[0],
+            out_small,
+            out_large,
+            residual,
+            norm_gain,
+            gate_weight,
+            up_weight,
+            down_weight,
+        )
     packed = pack(
         (key_small, value_small, key_large, value_large),
         jnp.concatenate([offset_small, offset_large], axis=0),
@@ -313,10 +875,9 @@
     gate_full = lax.all_gather(gate_weight, "sp", axis=0, tiled=True)
     up_full = lax.all_gather(up_weight, "sp", axis=0, tiled=True)
     down_full = lax.all_gather(down_weight, "sp", axis=1, tiled=True)
-    query = jnp.concatenate([query_small, query_large], axis=1)
     out_rows = jnp.concatenate([out_small, out_large], axis=0)
     mixed = attend(
-        n_sp, width, query, packed, offset_small.shape[0], offset_large.shape[0]
+        n_sp, width, query_small, query_large, packed, offset_small.shape[0], offset_large.shape[0]
     )
     attended = lax.psum_scatter(
         jnp.dot(mixed, out_rows, preferred_element_type=jnp.float32).astype(jnp.bfloat16),

time: 626 us -> 340 us (0.54)
  waiting for transfers between devices: 413 us -> 0 us
  Pallas kernels: 157 us -> 333 us
  matrix products: 30 us -> 0 us
  between operations: 15.1 us -> 0.01 us
    all_gather x4 -> x0, waiting for transfers between devices: 256 us -> none  [the longest x1 92.5 us: layer(): up_full = lax.all_gather(up_weight, 'sp', axis=0, tiled=True)]
    pallas_call x1, Pallas kernels: 157 us -> 333 us  [fused_layer(): pl.pallas_call(functools.partial(layer_kernel, n_sp, width, n_small, n_la...]
    reduce_scatter x2 -> x0, waiting for transfers between devices: 155 us -> none  [the longest x1 118 us: layer(): lax.psum_scatter(jnp.dot(mixed, out_rows, preferred_element_type=jnp.floa...]
    dot_general x3 -> x0, matrix products: 30 us -> none  [the longest x1 16.8 us: layer(): jnp.dot(hidden, down_full, preferred_element_type=jnp.float32)]
  transfers between devices with their start and end apart: 6 -> 0, of which waited for: 6 -> 0; matrix products, arithmetic and copies ran while one was open for 2% -> 0% of each run, Pallas kernels for 0% -> 0%
where the time goes in v1:
time: 340 us
  Pallas kernels  333 us (98%)
  other arithmetic  3.47 us (1%)
    pallas_call x1, Pallas kernels, fused_layer(): pl.pallas_call(functools.partial(layer_kernel, n_sp, width, n_small, n_la...  333 us

profile of v1, /device:TPU:16, one launch (start us, length us, event | category | flops | bytes accessed | tf_op | source)
XLA Modules:
  0.0 339.6 jit_solution(6831971644901290342)
XLA Ops:
  0.0 1.3 reshape.3.gain_ref
  1.3 0.7 fusion.5
  2.0 2.7 pad_maximum_fusion.own_ref
  4.8 332.8 %fused_layer.1 = bf16[192,2048]{1,0:T(8,128)(2,1)} custom-call(bf16[768,256]{1,0:T(8,128)(2,1)} %small_ref.1, bf16[768,256]{1,0:T(8,128)(2,1)} %large_ref.1, bf16[784,1024]{1,0:T(8,128)(2,1)} %pad_maximum_fusion.own_ref, bf16[256,2048]{1,0:T(8,128)(2,1)} %out_small_ref.1, bf16[256,2048]{1,0:T(8,128)(2,1)} %out_large_ref.1, bf16[192,2048]{1,0:T(8,128)(2,1)} %residual_ref.1, ...), custom_call_target="tpu_custom_call" | custom-call | tf_op jit(solution)/shard_map/fused_layer/pallas_call | solution.py:768
  337.5 2.1 copy.17

commit v2 on v1

--- a/solution.py
+++ b/solution.py
@@ -218,7 +218,8 @@
 
             wanted = (column != self.x) & ((row < self.z) | (column > self.x))
             if self.shifted:
-                wanted &= (row > 0) | (self.z == 0) | (self.x > 0)
+                last = self.z == self.n_sp // self.width - 1
+                wanted &= (row > 0) | ~last | (self.x > 0)
 
             @pl.when(wanted)
             def _(column=column):
@@ -533,7 +534,7 @@
     def landed(block):
         @pl.when((block == 0) & (x == 1))
         def _():
-            @pl.when(z < height - 1)
+            @pl.when(z == height - 2)
             def _():
                 shift_copy().start()
 
@@ -712,7 +713,7 @@
 
     travel.finish()
 
-    @pl.when((x == 1) & (z < height - 1))
+    @pl.when((x == 1) & (z == height - 2))
     def _():
         shift_copy().wait_send()
 

time: 340 us -> 337 us (level)
  no operation moved by 1% of the time
where the time goes in v2:
time: 337 us
  Pallas kernels  330 us (98%)
  other arithmetic  3.47 us (1%)
  local copies, waits for them, and re-layouts  3.38 us (1%)
    pallas_call x1, Pallas kernels, fused_layer(): pl.pallas_call(functools.partial(layer_kernel, n_sp, width, n_small, n_la...  330 us

profile of v2, /device:TPU:16, one launch (start us, length us, event | category | flops | bytes accessed | tf_op | source)
XLA Modules:
  0.0 337.1 jit_solution(14942036624811662944)
XLA Ops:
  0.0 1.3 reshape.3.gain_ref
  1.3 0.7 fusion.5
  2.0 2.7 pad_maximum_fusion.own_ref
  4.8 330.2 %fused_layer.1 = bf16[192,2048]{1,0:T(8,128)(2,1)} custom-call(bf16[768,256]{1,0:T(8,128)(2,1)} %small_ref.1, bf16[768,256]{1,0:T(8,128)(2,1)} %large_ref.1, bf16[784,1024]{1,0:T(8,128)(2,1)} %pad_maximum_fusion.own_ref, bf16[256,2048]{1,0:T(8,128)(2,1)} %out_small_ref.1, bf16[256,2048]{1,0:T(8,128)(2,1)} %out_large_ref.1, bf16[192,2048]{1,0:T(8,128)(2,1)} %residual_ref.1, ...), custom_call_target="tpu_custom_call" | custom-call | tf_op jit(solution)/shard_map/fused_layer/pallas_call | solution.py:769
  335.0 2.1 copy.17
